TPU v7x, 32 devices: a whole 2x2x4 slice. The times are simulated.
32 devices in a mesh: ep: 8 (over z, core), tp: 4 (over y, x).
Axes of the slice: x: 2, y: 2, z: 4, core: 2. Of those that a mesh axis runs over, the one named last changes fastest.
Arguments:
- tokens: bfloat16 [1024, 4096], P('ep', 'tp'), may hold values from -6 to 6
- out_grad: bfloat16 [1024, 4096], P('ep', 'tp'), may hold values from -1.5 to 1.5
- routes: int32 [1024, 2], P('ep'), may hold values from 0 to 7, all different within a row; in each aligned block of 128 rows (0 to 127, 128 to 255, ...) at most 40 rows name the same one
- route_weights: float32 [1024, 2], P('ep'), may hold values from 0.2 to 1.2
- gate_proj: bfloat16 [8, 1024, 4096], P('ep', 'tp'), may hold values from -0.09375 to 0.09375
- up_proj: bfloat16 [8, 1024, 4096], P('ep', 'tp'), may hold values from -0.09375 to 0.09375
- down_proj: bfloat16 [8, 1024, 4096], P('ep', 'tp'), may hold values from -0.1875 to 0.1875
- shared_hidden: bfloat16 [1024, 1024], P('ep'), may hold values from -6 to 6
Outputs:
- token_grad: bfloat16 [1024, 4096], P('ep', 'tp')
- weight_grad: float32 [1024, 2], P('ep')
- gate_grad: bfloat16 [8, 1024, 4096], P('ep', 'tp')
- up_grad: bfloat16 [8, 1024, 4096], P('ep', 'tp')
- down_grad: bfloat16 [8, 1024, 4096], P('ep', 'tp')
- shared_grad: float32 [1024, 4096], P('ep', 'tp')
Inputs may be any that keep to these rules, and one draw needn't show every extreme that they name: Within each block of 128 consecutive tokens, no expert is named by more than 40 routes, and in some blocks one expert is named by exactly 40. The 2 experts of one token differ.
All inputs are finite; a program needn't handle non-finite values.
Results may differ from a plain program's by a relative error of at most 0.0065.
Values may be sent and summed in bfloat16 or wider, within the bound.
A program may use at most 64 MiB of HBM per device.

v0:
```python
import jax
import jax.numpy as jnp
from jax import lax
from jax.sharding import PartitionSpec as P


def slot_tables(routes, num_experts, capacity):
    tok_rows, per_token = routes.shape
    route_count = tok_rows * per_token
    flat_routes = routes.reshape(-1)
    expert_ids = lax.broadcasted_iota(jnp.int32, (route_count, num_experts), 1)
    onehot = (flat_routes[:, None] == expert_ids).astype(jnp.int32)
    slot_rank = jnp.sum((jnp.cumsum(onehot, axis=0) - 1) * onehot, axis=1)
    slot_of_route = flat_routes * capacity + slot_rank
    slot_ids = lax.broadcasted_iota(jnp.int32, (num_experts * capacity, route_count), 0)
    route_ids = lax.broadcasted_iota(jnp.int32, (num_experts * capacity, route_count), 1)
    matches = slot_ids == slot_of_route[None, :]
    route_of_slot = jnp.sum(jnp.where(matches, route_ids, 0), axis=1)
    filled = jnp.any(matches, axis=1)
    return (slot_of_route, route_of_slot, filled)


def local(tokens, out_grad, routes, route_weights, gate_proj, up_proj, down_proj, shared_hidden):
    ep_count = lax.axis_size("ep")
    tp_count = lax.axis_size("tp")
    local_experts = gate_proj.shape[0]
    num_experts = local_experts * ep_count
    tok_rows, per_token = routes.shape
    capacity = max(2, 5 * tok_rows * per_token // (4 * num_experts))
    slot_of_route, route_of_slot, filled = slot_tables(routes, num_experts, capacity)
    token_of_slot = route_of_slot // per_token
    zero_value = jnp.zeros((), jnp.bfloat16)
    slot_weight = jnp.where(filled, route_weights.reshape(-1)[route_of_slot], 0.0)
    slot_weight = slot_weight.astype(jnp.bfloat16).reshape(ep_count, local_experts, capacity)
    layout = (ep_count, local_experts, capacity, -1)
    sent_tokens = jnp.where(filled[:, None], tokens[token_of_slot], zero_value).reshape(layout)
    sent_grads = jnp.where(filled[:, None], out_grad[token_of_slot], zero_value).reshape(layout)
    part_tokens, part_grads, weights_in = (
        lax.all_to_all(sent_tokens, "ep", split_axis=0, concat_axis=2, tiled=True),
        lax.all_to_all(sent_grads, "ep", split_axis=0, concat_axis=2, tiled=True),
        lax.all_to_all(slot_weight, "ep", split_axis=0, concat_axis=2, tiled=True),
    )
    rows_in, grads_in = (
        lax.all_gather(part_tokens, "tp", axis=3, tiled=True),
        lax.all_gather(part_grads, "tp", axis=3, tiled=True),
    )
    rows_in = rows_in[0]
    grads_in = grads_in[0]
    slot_scale = weights_in[0].astype(jnp.float32)
    pre_gate = jnp.einsum("lrd,lfd->lrf", rows_in, gate_proj, preferred_element_type=jnp.float32)
    pre_up = jnp.einsum("lrd,lfd->lrf", rows_in, up_proj, preferred_element_type=jnp.float32)
    squash = jax.nn.sigmoid(pre_gate)
    activated = pre_gate * squash
    hidden = (activated * pre_up).astype(jnp.bfloat16)
    back_grad = jnp.einsum("lrd,lfd->lrf", grads_in, down_proj, preferred_element_type=jnp.float32)
    partial_products = jnp.sum(hidden.astype(jnp.float32) * back_grad, axis=2)
    hidden_grad = slot_scale[:, :, None] * back_grad
    scaled_hidden = (slot_scale[:, :, None] * hidden.astype(jnp.float32)).astype(jnp.bfloat16)
    gate_delta = (hidden_grad * pre_up * squash * (1.0 + pre_gate * (1.0 - squash))).astype(
        jnp.bfloat16
    )
    up_delta = (hidden_grad * activated).astype(jnp.bfloat16)
    gate_grad = jnp.einsum(
        "lrf,lrd->lfd", gate_delta, rows_in, preferred_element_type=jnp.float32
    ).astype(jnp.bfloat16)
    up_grad = jnp.einsum(
        "lrf,lrd->lfd", up_delta, rows_in, preferred_element_type=jnp.float32
    ).astype(jnp.bfloat16)
    down_grad = jnp.einsum(
        "lrf,lrd->lfd", scaled_hidden, grads_in, preferred_element_type=jnp.float32
    ).astype(jnp.bfloat16)
    partial_rows = jnp.einsum(
        "lrf,lfd->lrd", gate_delta, gate_proj, preferred_element_type=jnp.float32
    )
    partial_rows = partial_rows + jnp.einsum(
        "lrf,lfd->lrd", up_delta, up_proj, preferred_element_type=jnp.float32
    )
    partial_rows = partial_rows.astype(jnp.bfloat16)
    gathered = lax.all_to_all(partial_rows, "tp", split_axis=2, concat_axis=0, tiled=True)
    gathered = gathered.reshape((tp_count,) + partial_rows.shape[:2] + (-1,))
    summed = jnp.sum(gathered, axis=0, dtype=jnp.float32)
    products = lax.psum(partial_products, "tp")
    slot_rows, slot_products = (
        lax.all_to_all(summed[None], "ep", split_axis=2, concat_axis=0, tiled=True),
        lax.all_to_all(products[None], "ep", split_axis=2, concat_axis=0, tiled=True),
    )
    feature_width = slot_rows.shape[-1]
    slot_rows = slot_rows.reshape(num_experts * capacity, feature_width)
    route_rows = slot_rows[slot_of_route].reshape(tok_rows, per_token, feature_width)
    token_grad = jnp.sum(route_rows, axis=1).astype(jnp.bfloat16)
    weight_grad = slot_products.reshape(-1)[slot_of_route].reshape(tok_rows, per_token)
    shared_grad = lax.psum_scatter(
        lax.dot_general(
            shared_hidden, out_grad, (((0,), (0,)), ((), ())), preferred_element_type=jnp.float32
        ),
        "ep",
        scatter_dimension=0,
        tiled=True,
    )
    return (token_grad, weight_grad, gate_grad, up_grad, down_grad, shared_grad)


def solution(mesh):
    return jax.shard_map(
        local,
        mesh=mesh,
        in_specs=(
            P("ep", "tp"),
            P("ep", "tp"),
            P("ep", None),
            P("ep", None),
            P("ep", "tp", None),
            P("ep", "tp", None),
            P("ep", "tp", None),
            P("ep", None),
        ),
        out_specs=(
            P("ep", "tp"),
            P("ep", None),
            P("ep", "tp", None),
            P("ep", "tp", None),
            P("ep", "tp", None),
            P("ep", "tp"),
        ),
        check_vma=False,
    )
```

profile of v0, /device:TPU:0, one launch (start us, length us, event | category | flops | bytes accessed | tf_op | source)
XLA Modules:
  0.0 350.5 jit_solution(12991959504227618092)
XLA Ops:
  8.1 1.0 copy.50
  9.3 0.6 reduce-window.6
  9.9 0.2 slice_reduce_fusion
  10.3 0.2 select_reduce_fusion
  10.4 0.2 fusion.23
  10.6 2.6 gather_fusion.1
  13.3 2.6 gather_fusion.2
  16.0 1.4 broadcast_select_fusion.1
  17.5 24.5 %all_to_all.60 = bf16[8,1,40,1024]{3,2,1,0:T(8,128)(2,1)} all-to-all(bf16[8,1,40,1024]{3,2,1,0:T(8,128)(2,1)S(1)} %get-tuple-element.43), channel_id=1, replica_groups=mesh['ep'=8,'tp'=4] {'ep'}, dimensions={0} | all-to-all | bytes 1310720 | tf_op jit(solution)/shard_map/all_to_all | solution.py:39
  42.1 21.2 %all_to_all.61 = bf16[8,1,40,1024]{3,2,1,0:T(8,128)(2,1)} all-to-all(bf16[8,1,40,1024]{3,2,1,0:T(8,128)(2,1)S(1)} %get-tuple-element.42), channel_id=1, replica_groups=mesh['ep'=8,'tp'=4] {'ep'}, dimensions={0} | all-to-all | bytes 1310720 | tf_op jit(solution)/shard_map/all_to_all | solution.py:40
  63.4 2.8 fusion.30
  66.2 0.7 copy-done.10
  67.1 2.4 gather_fusion
  69.6 8.1 %all_to_all.62 = bf16[8,1,40]{2,1,0:T(2,128)(2,1)S(1)} all-to-all(bf16[8,1,40]{2,1,0:T(2,128)(2,1)S(1)} %convert_element_type.110), channel_id=1, replica_groups=mesh['ep'=8,'tp'=4] {'ep'}, dimensions={0} | all-to-all | bytes 1280 | tf_op jit(solution)/shard_map/all_to_all | solution.py:41
  77.8 2.8 all-gather.5.cloned.1.call-done
  80.6 2.8 fusion.7
  83.4 0.4 copy-done.6
  83.9 0.9 fusion.9
  84.8 37.3 %all-gather.3.cloned.1.call-done = bf16[1,1,320,4096]{3,2,1,0:T(8,128)(2,1)} async-done(((bf16[1,1,320,1024]{3,2,1,0:T(8,128)(2,1)}), bf16[1,1,320,4096]{3,2,1,0:T(8,128)(2,1)}) %all-gather.3.cloned.1.call-update) | async-done | bytes 2621456 | tf_op jit(solution)/shard_map/all_gather | solution.py:45
  122.0 3.4 fusion.20
  125.4 0.8 fusion.14
  126.3 0.7 copy-done.7
  127.0 2.4 fusion.1
  129.4 14.3 %copy.56 = bf16[1,320,4096]{1,0,2:T(2,128)(2,1)} copy(bf16[1,320,4096]{2,1,0:T(8,128)(2,1)} %fusion.1) | data formatting | bytes 5242880 | tf_op jit(solution)/shard_map/convert_element_type | solution.py:78
  143.7 0.5 broadcast.230
  144.3 68.8 %reduce.16 = bf16[4096,320]{1,0:T(8,128)(2,1)} reduce(bf16[4096,1,320]{2,1,0:T(2,128)(2,1)} %bitcast.67, bf16[]{:T(256)} %broadcast.230), dimensions={1}, to_apply=%bitcast.53.reduce_sub_computation | reduce | bytes 5242882
  213.0 6.1 %reshape.388 = bf16[4,2,163840]{2,1,0:T(2,128)(2,1)} reshape(bf16[4096,320]{1,0:T(8,128)(2,1)} %reduce.16) | data formatting | bytes 5242880
  219.2 4.6 %all-to-all-start.3 = ((bf16[4,2,163840]{2,1,0:T(2,128)(2,1)}), bf16[4,2,163840]{2,1,0:T(2,128)(2,1)}, u32[]{:S(2)}, u32[]{:S(2)}) async-start(bf16[4,2,163840]{2,1,0:T(2,128)(2,1)} %reshape.388), calls=%async_computation.3 | async-start | bytes 5242880 | tf_op jit(solution)/shard_map/all_to_all | solution.py:79
  223.8 33.7 %psum.7 = f32[1,1,320]{2,1,0:T(1,128)S(1)} all-reduce(f32[1,1,320]{2,1,0:T(1,128)S(1)} %broadcast_in_dim.48), channel_id=1, replica_groups=mesh['ep'=8,'tp'=4] {'tp'}, use_global_device_ids=true, to_apply=%region_8.9 | all-reduce | flops 320 | bytes 2560 | tf_op jit(solution)/shard_map/psum | solution.py:82
  257.5 0.8 copy.59
  258.3 4.6 %all-to-all-start.5 = ((f32[1,1,320]{1,0,2:T(1,128)}), f32[1,1,320]{1,0,2:T(1,128)S(1)}, u32[]{:S(2)}, u32[]{:S(2)}) async-start(f32[1,1,320]{1,0,2:T(1,128)} %copy.59), calls=%async_computation.5 | async-start | bytes 327680 | tf_op jit(solution)/shard_map/all_to_all | solution.py:85
  262.9 7.6 %reshape.389 = bf16[4096,1,320]{2,1,0:T(2,128)(2,1)} reshape(bf16[4,2,163840]{2,1,0:T(2,128)(2,1)} %all-to-all-done.3) | data formatting | bytes 5242880
  270.5 14.0 %copy.57 = bf16[1,320,4096]{2,1,0:T(8,128)(2,1)} copy(bf16[1,320,4096]{1,0,2:T(2,128)(2,1)} %bitcast.68) | data formatting | bytes 5242880 | tf_op jit(solution)/shard_map/all_to_all | solution.py:79
  284.5 7.3 %reshape.336 = f32[320,4,1024]{2,1,0:T(4,128)} reshape(bf16[1,320,4096]{2,1,0:T(8,128)(2,1)} %copy.57) | data formatting | bytes 7864320 | tf_op jit(solution)/shard_map/convert_element_type | solution.py:81
  291.8 5.7 %reduce_sum.54 = f32[320,1024]{1,0:T(8,128)S(1)} reduce(f32[320,4,1024]{2,1,0:T(4,128)} %reshape.336, f32[]{:T(128)} %constant.33.clone.1), dimensions={1}, to_apply=%region_5.6 | reduce | flops 983040 | bytes 6553604 | tf_op jit(solution)/shard_map/reduce_sum | solution.py:81
  297.5 2.0 broadcast_in_dim.47
  299.5 5.1 %all-to-all-start.4 = ((f32[1,1,320,1024]{3,1,0,2:T(1,128)}), f32[1,1,320,1024]{3,1,0,2:T(1,128)S(1)}, u32[]{:S(2)}, u32[]{:S(2)}) async-start(f32[1,1,320,1024]{3,1,0,2:T(1,128)} %broadcast_in_dim.47), calls=%async_computation.4 | async-start | bytes 2621440 | tf_op jit(solution)/shard_map/all_to_all | solution.py:84
  304.9 4.3 %fusion.2 = bf16[1,256,4096]{2,1,0:T(8,128)(2,1)} fusion(bf16[320,256]{1,0:T(8,128)(2,1)S(1)} %get-tuple-element.40, bf16[1,1,320,4096]{3,2,1,0:T(8,128)(2,1)} %all-gather.5.cloned.1.call-done), kind=kOutput, calls=%fused_computation.11 | convolution fusion | flops 672137216 | bytes 4882432 | tf_op jit(solution)/shard_map/lrf,lrd->lfd/dot_general | solution.py:63
  309.3 4.5 %fusion.3 = bf16[1,256,4096]{2,1,0:T(8,128)(2,1)} fusion(bf16[320,256]{1,0:T(8,128)(2,1)S(1)} %get-tuple-element.41, bf16[1,1,320,4096]{3,2,1,0:T(8,128)(2,1)} %all-gather.5.cloned.1.call-done), kind=kOutput, calls=%fused_computation.12 | convolution fusion | flops 672137216 | bytes 4882432 | tf_op jit(solution)/shard_map/lrf,lrd->lfd/dot_general | solution.py:66
  313.7 2.7 fusion.4
  316.4 1.1 reduce.9
  317.5 1.9 gather_fusion.4
  319.6 0.6 copy.60
  320.2 16.6 %all-to-all-done.4 = f32[1,1,320,1024]{3,1,0,2:T(1,128)S(1)} async-done(((f32[1,1,320,1024]{3,1,0,2:T(1,128)}), f32[1,1,320,1024]{3,1,0,2:T(1,128)S(1)}, u32[]{:S(2)}, u32[]{:S(2)}) %all-to-all-start.4) | async-done | bytes 1310752 | tf_op jit(solution)/shard_map/all_to_all | solution.py:84
  336.8 0.3 copy.63
  337.1 2.0 gather_fusion.3
  339.1 1.8 reshape.331
  341.0 2.1 reduce_sum.56
  (51 shorter events, 1.6 us)
Async XLA Ops:
  8.0 72.6 %copy-start = (bf16[1,256,4096]{2,1,0:T(8,128)(2,1)S(1)}, bf16[1,256,4096]{2,1,0:T(8,128)(2,1)}, u32[]{:S(2)}) copy-start(bf16[1,256,4096]{2,1,0:T(8,128)(2,1)} %param.12) | copy-start | bytes 6291460
  8.0 2.6 copy-start.2
  8.0 72.6 %all-gather.5.cloned.1.call-start = ((), (), s32[]{:S(2)}) async-start(), calls=%async_computation.8 | async-start | bytes 3276800 | tf_op jit(solution)/shard_map/all_gather | solution.py:44
  10.6 2.7 copy-start.3
  17.5 45.9 %copy-start.8 = (bf16[128,1024]{1,0:T(8,128)(2,1)S(1)}, bf16[128,1024]{1,0:T(8,128)(2,1)}, u32[]{:S(2)}) copy-start(bf16[128,1024]{1,0:T(8,128)(2,1)} %param.15) | copy-start | bytes 786436
  42.0 80.0 %all-gather.3.cloned.1.call-start = ((), (), s32[]{:S(2)}) async-start(), calls=%async_computation.7 | async-start | bytes 3276800 | tf_op jit(solution)/shard_map/all_gather | solution.py:45
  63.3 279.7 %reduce-scatter.2.cloned.1.call-start = ((), (), s32[]{:S(2)}) async-start(), calls=%async_computation.9 | async-start | bytes 4718592 | tf_op jit(solution)/shard_map/reduce_scatter | solution.py:92
  66.2 0.7 copy-start.10
  80.6 2.8 copy-start.4
  80.6 3.2 copy-start.6
  125.4 1.6 copy-start.7
  219.2 39.1 %all-to-all-start.3 = ((bf16[4,2,163840]{2,1,0:T(2,128)(2,1)}), bf16[4,2,163840]{2,1,0:T(2,128)(2,1)}, u32[]{:S(2)}, u32[]{:S(2)}) async-start(bf16[4,2,163840]{2,1,0:T(2,128)(2,1)} %reshape.388), calls=%async_computation.3 | async-start | bytes 5242880 | tf_op jit(solution)/shard_map/all_to_all | solution.py:79
  258.3 41.2 %all-to-all-start.5 = ((f32[1,1,320]{1,0,2:T(1,128)}), f32[1,1,320]{1,0,2:T(1,128)S(1)}, u32[]{:S(2)}, u32[]{:S(2)}) async-start(f32[1,1,320]{1,0,2:T(1,128)} %copy.59), calls=%async_computation.5 | async-start | bytes 327680 | tf_op jit(solution)/shard_map/all_to_all | solution.py:85
  297.5 7.1 %copy-start.9 = (s32[128,2]{0,1:T(2,128)S(1)}, s32[128,2]{0,1:T(2,128)}, u32[]{:S(2)}) copy-start(s32[128,2]{0,1:T(2,128)} %param.10) | copy-start | bytes 3076
  299.5 37.3 %all-to-all-start.4 = ((f32[1,1,320,1024]{3,1,0,2:T(1,128)}), f32[1,1,320,1024]{3,1,0,2:T(1,128)S(1)}, u32[]{:S(2)}, u32[]{:S(2)}) async-start(f32[1,1,320,1024]{3,1,0,2:T(1,128)} %broadcast_in_dim.47), calls=%async_computation.4 | async-start | bytes 2621440 | tf_op jit(solution)/shard_map/all_to_all | solution.py:84
  309.3 4.5 %copy-start.5 = (bf16[1,1,320,4096]{3,2,1,0:T(8,128)(2,1)S(1)}, bf16[1,1,320,4096]{3,2,1,0:T(8,128)(2,1)}, u32[]{:S(2)}) copy-start(bf16[1,1,320,4096]{3,2,1,0:T(8,128)(2,1)} %all-gather.3.cloned.1.call-done) | copy-start | bytes 7864324
  337.1 6.0 %copy-start.1 = (bf16[1,256,4096]{2,1,0:T(8,128)(2,1)S(1)}, bf16[1,256,4096]{2,1,0:T(8,128)(2,1)}, u32[]{:S(2)}) copy-start(bf16[1,256,4096]{2,1,0:T(8,128)(2,1)} %param.12) | copy-start | bytes 6291460
Sparse Core Ops, SparseCore 0:
  42.1 38.4 all-gather.4
  82.5 39.4 all-gather.2
Sparse Core Ops, SparseCore 1:
  66.7 48.8 reduce-scatter.1
where the time goes:
time: 352 us; the launch traced here: 350 us
  blocking collectives  87.6 us (25%)
  other arithmetic  80.1 us (23%)
  local copies, waits for them, and re-layouts  71.3 us (20%)
  waiting for transfers between devices  56.7 us (16%)
  matrix products  24.6 us (7%)
  between operations  15.7 us (4%)
  starting transfers between devices  14.4 us (4%)
    unnamed x1, other arithmetic  68.8 us
    all_gather x1, waiting for transfers between devices, local(): lax.all_gather(part_grads, 'tp', axis=3, tiled=True)  37.3 us
    psum x1, blocking collectives, local(): products = lax.psum(partial_products, 'tp')  33.7 us
    all_to_all x1, blocking collectives, local(): lax.all_to_all(sent_tokens, 'ep', split_axis=0, concat_axis=2, tiled=True)  24.5 us
    all_to_all x1, blocking collectives, local(): lax.all_to_all(sent_grads, 'ep', split_axis=0, concat_axis=2, tiled=True)  21.2 us
    unnamed x29, local copies, waits for them, and re-layouts  18.1 us
    all_to_all x1, waiting for transfers between devices, local(): lax.all_to_all(summed[None], 'ep', split_axis=2, concat_axis=0, tiled=True)  16.6 us
    convert_element_type x1, local copies, waits for them, and re-layouts, local(): partial_rows = partial_rows.astype(jnp.bfloat16)  14.3 us
  transfers between devices with their start and end apart: 6, of which 3 were waited for; matrix products, arithmetic and copies ran while one was open for 47% of the time, Pallas kernels for 0%

commit v1 on v0

--- a/solution.py
+++ b/solution.py
@@ -2,6 +2,15 @@
 import jax.numpy as jnp
 from jax import lax
 from jax.sharding import PartitionSpec as P
+
+
+def add_in_pairs(x, axis):
+    size = lax.axis_size(axis)
+    result, far = (x, 1)
+    while far < size:
+        result = result + lax.ppermute(result, axis, [(i, i ^ far) for i in range(size)])
+        far = 2 * far
+    return result
 
 
 def slot_tables(routes, num_experts, capacity):
@@ -79,7 +88,7 @@
     gathered = lax.all_to_all(partial_rows, "tp", split_axis=2, concat_axis=0, tiled=True)
     gathered = gathered.reshape((tp_count,) + partial_rows.shape[:2] + (-1,))
     summed = jnp.sum(gathered, axis=0, dtype=jnp.float32)
-    products = lax.psum(partial_products, "tp")
+    products = add_in_pairs(partial_products, "tp")
     slot_rows, slot_products = (
         lax.all_to_all(summed[None], "ep", split_axis=2, concat_axis=0, tiled=True),
         lax.all_to_all(products[None], "ep", split_axis=2, concat_axis=0, tiled=True),

time: 352 us -> 353 us (level)
  blocking collectives: 87.6 us -> 53.9 us
  waiting for transfers between devices: 56.7 us -> 87.5 us
    psum x1 -> x0, blocking collectives: 33.7 us -> none  [local(): products = lax.psum(partial_products, 'tp')]
    ppermute x0 -> x2, waiting for transfers between devices: none -> 30.8 us  [add_in_pairs(): lax.ppermute(result, axis, [(i, i ^ far) for i in range(size)])]
  transfers between devices with their start and end apart: 6 -> 8, of which waited for: 3 -> 5; matrix products, arithmetic and copies ran while one was open for 47% -> 47% of each run, Pallas kernels for 0% -> 0%
where the time goes in v1:
time: 353 us; the launch traced here: 351 us
  waiting for transfers between devices  87.5 us (25%)
  other arithmetic  80.1 us (23%)
  local copies, waits for them, and re-layouts  71.3 us (20%)
  blocking collectives  53.9 us (15%)
  matrix products  24.6 us (7%)
  starting transfers between devices  17.8 us (5%)
  between operations  15.7 us (4%)
    unnamed x1, other arithmetic  68.8 us
    all_gather x1, waiting for transfers between devices, local(): lax.all_gather(part_grads, 'tp', axis=3, tiled=True)  37.3 us
    ppermute x2, waiting for transfers between devices, add_in_pairs(): lax.ppermute(result, axis, [(i, i ^ far) for i in range(size)])  30.8 us
    all_to_all x1, blocking collectives, local(): lax.all_to_all(sent_tokens, 'ep', split_axis=0, concat_axis=2, tiled=True)  24.5 us
    all_to_all x1, blocking collectives, local(): lax.all_to_all(sent_grads, 'ep', split_axis=0, concat_axis=2, tiled=True)  21.2 us
    unnamed x29, local copies, waits for them, and re-layouts  18.1 us
    all_to_all x1, waiting for transfers between devices, local(): lax.all_to_all(summed[None], 'ep', split_axis=2, concat_axis=0, tiled=True)  16.6 us
    convert_element_type x1, local copies, waits for them, and re-layouts, local(): partial_rows = partial_rows.astype(jnp.bfloat16)  14.3 us
  transfers between devices with their start and end apart: 8, of which 5 were waited for; matrix products, arithmetic and copies ran while one was open for 47% of the time, Pallas kernels for 0%

profile of v1, /device:TPU:0, one launch (start us, length us, event | category | flops | bytes accessed | tf_op | source)
XLA Modules:
  0.0 351.0 jit_solution(6714992095780923295)
XLA Ops:
  8.1 1.0 copy.50
  9.3 0.6 reduce-window.6
  10.6 2.6 gather_fusion.1
  13.3 2.6 gather_fusion.2
  16.0 1.4 broadcast_select_fusion.1
  17.5 24.5 %all_to_all.60 = bf16[8,1,40,1024]{3,2,1,0:T(8,128)(2,1)} all-to-all(bf16[8,1,40,1024]{3,2,1,0:T(8,128)(2,1)S(1)} %get-tuple-element.43), channel_id=1, replica_groups=mesh['ep'=8,'tp'=4] {'ep'}, dimensions={0} | all-to-all | bytes 1310720 | tf_op jit(solution)/shard_map/all_to_all | solution.py:48
  42.1 21.2 %all_to_all.61 = bf16[8,1,40,1024]{3,2,1,0:T(8,128)(2,1)} all-to-all(bf16[8,1,40,1024]{3,2,1,0:T(8,128)(2,1)S(1)} %get-tuple-element.42), channel_id=1, replica_groups=mesh['ep'=8,'tp'=4] {'ep'}, dimensions={0} | all-to-all | bytes 1310720 | tf_op jit(solution)/shard_map/all_to_all | solution.py:49
  63.4 2.8 fusion.30
  66.2 0.7 copy-done.10
  67.1 2.4 gather_fusion
  69.6 8.1 %all_to_all.62 = bf16[8,1,40]{2,1,0:T(2,128)(2,1)S(1)} all-to-all(bf16[8,1,40]{2,1,0:T(2,128)(2,1)S(1)} %convert_element_type.110), channel_id=1, replica_groups=mesh['ep'=8,'tp'=4] {'ep'}, dimensions={0} | all-to-all | bytes 1280 | tf_op jit(solution)/shard_map/all_to_all | solution.py:50
  77.8 2.8 all-gather.5.cloned.1.call-done
  80.6 2.8 fusion.7
  83.4 0.4 copy-done.6
  83.9 0.9 fusion.9
  84.8 37.3 %all-gather.3.cloned.1.call-done = bf16[1,1,320,4096]{3,2,1,0:T(8,128)(2,1)} async-done(((bf16[1,1,320,1024]{3,2,1,0:T(8,128)(2,1)}), bf16[1,1,320,4096]{3,2,1,0:T(8,128)(2,1)}) %all-gather.3.cloned.1.call-update) | async-done | bytes 2621456 | tf_op jit(solution)/shard_map/all_gather | solution.py:54
  122.0 3.4 fusion.20
  125.4 0.8 fusion.14
  126.3 0.7 copy-done.7
  127.0 2.4 fusion.1
  129.4 14.3 %copy.56 = bf16[1,320,4096]{1,0,2:T(2,128)(2,1)} copy(bf16[1,320,4096]{2,1,0:T(8,128)(2,1)} %fusion.1) | data formatting | bytes 5242880 | tf_op jit(solution)/shard_map/convert_element_type | solution.py:87
  143.7 0.5 broadcast.230
  144.3 68.8 %reduce.16 = bf16[4096,320]{1,0:T(8,128)(2,1)} reduce(bf16[4096,1,320]{2,1,0:T(2,128)(2,1)} %bitcast.69, bf16[]{:T(256)} %broadcast.230), dimensions={1}, to_apply=%bitcast.55.reduce_sub_computation | reduce | bytes 5242882
  213.0 6.1 %reshape.387 = bf16[4,2,163840]{2,1,0:T(2,128)(2,1)} reshape(bf16[4096,320]{1,0:T(8,128)(2,1)} %reduce.16) | data formatting | bytes 5242880
  219.2 4.8 %all-to-all-start.3 = ((bf16[4,2,163840]{2,1,0:T(2,128)(2,1)}), bf16[4,2,163840]{2,1,0:T(2,128)(2,1)}, u32[]{:S(2)}, u32[]{:S(2)}) async-start(bf16[4,2,163840]{2,1,0:T(2,128)(2,1)} %reshape.387), calls=%async_computation.3 | async-start | bytes 5242880 | tf_op jit(solution)/shard_map/all_to_all | solution.py:88
  224.0 1.7 collective-permute-start
  225.7 28.7 %collective-permute-done = f32[1,320]{1,0:T(1,128)S(1)} collective-permute-done((f32[1,320]{1,0:T(1,128)S(1)}, f32[1,320]{1,0:T(1,128)S(1)}, u32[]{:S(2)}, u32[]{:S(2)}) %collective-permute-start) | collective-permute-done | bytes 1312 | tf_op jit(solution)/shard_map/ppermute | solution.py:11
  254.4 1.5 collective-permute-start.1
  255.9 2.1 collective-permute-done.1
  258.0 0.8 copy.59
  258.9 4.6 %all-to-all-start.5 = ((f32[1,1,320]{1,0,2:T(1,128)}), f32[1,1,320]{1,0,2:T(1,128)S(1)}, u32[]{:S(2)}, u32[]{:S(2)}) async-start(f32[1,1,320]{1,0,2:T(1,128)} %copy.59), calls=%async_computation.5 | async-start | bytes 327680 | tf_op jit(solution)/shard_map/all_to_all | solution.py:94
  263.5 7.6 %reshape.388 = bf16[4096,1,320]{2,1,0:T(2,128)(2,1)} reshape(bf16[4,2,163840]{2,1,0:T(2,128)(2,1)} %all-to-all-done.3) | data formatting | bytes 5242880
  271.1 14.0 %copy.57 = bf16[1,320,4096]{2,1,0:T(8,128)(2,1)} copy(bf16[1,320,4096]{1,0,2:T(2,128)(2,1)} %bitcast.70) | data formatting | bytes 5242880 | tf_op jit(solution)/shard_map/all_to_all | solution.py:88
  285.0 7.3 %reshape.335 = f32[320,4,1024]{2,1,0:T(4,128)} reshape(bf16[1,320,4096]{2,1,0:T(8,128)(2,1)} %copy.57) | data formatting | bytes 7864320 | tf_op jit(solution)/shard_map/convert_element_type | solution.py:90
  292.4 5.7 %reduce_sum.54 = f32[320,1024]{1,0:T(8,128)S(1)} reduce(f32[320,4,1024]{2,1,0:T(4,128)} %reshape.335, f32[]{:T(128)} %constant.33.clone.1), dimensions={1}, to_apply=%region_5.6 | reduce | flops 983040 | bytes 6553604 | tf_op jit(solution)/shard_map/reduce_sum | solution.py:90
  298.1 2.0 broadcast_in_dim.47
  300.1 5.1 %all-to-all-start.4 = ((f32[1,1,320,1024]{3,1,0,2:T(1,128)}), f32[1,1,320,1024]{3,1,0,2:T(1,128)S(1)}, u32[]{:S(2)}, u32[]{:S(2)}) async-start(f32[1,1,320,1024]{3,1,0,2:T(1,128)} %broadcast_in_dim.47), calls=%async_computation.4 | async-start | bytes 2621440 | tf_op jit(solution)/shard_map/all_to_all | solution.py:93
  305.5 4.3 %fusion.2 = bf16[1,256,4096]{2,1,0:T(8,128)(2,1)} fusion(bf16[320,256]{1,0:T(8,128)(2,1)S(1)} %get-tuple-element.40, bf16[1,1,320,4096]{3,2,1,0:T(8,128)(2,1)} %all-gather.5.cloned.1.call-done), kind=kOutput, calls=%fused_computation.11 | convolution fusion | flops 672137216 | bytes 4882432 | tf_op jit(solution)/shard_map/lrf,lrd->lfd/dot_general | solution.py:72
  309.8 4.5 %fusion.3 = bf16[1,256,4096]{2,1,0:T(8,128)(2,1)} fusion(bf16[320,256]{1,0:T(8,128)(2,1)S(1)} %get-tuple-element.41, bf16[1,1,320,4096]{3,2,1,0:T(8,128)(2,1)} %all-gather.5.cloned.1.call-done), kind=kOutput, calls=%fused_computation.12 | convolution fusion | flops 672137216 | bytes 4882432 | tf_op jit(solution)/shard_map/lrf,lrd->lfd/dot_general | solution.py:75
  314.3 2.7 fusion.4
  317.0 1.1 reduce.9
  318.0 1.9 gather_fusion.4
  320.1 0.6 copy.60
  320.8 16.6 %all-to-all-done.4 = f32[1,1,320,1024]{3,1,0,2:T(1,128)S(1)} async-done(((f32[1,1,320,1024]{3,1,0,2:T(1,128)}), f32[1,1,320,1024]{3,1,0,2:T(1,128)S(1)}, u32[]{:S(2)}, u32[]{:S(2)}) %all-to-all-start.4) | async-done | bytes 1310752 | tf_op jit(solution)/shard_map/all_to_all | solution.py:93
  337.4 0.3 copy.63
  337.6 2.0 gather_fusion.3
  339.7 1.8 reshape.331
  341.5 2.1 reduce_sum.56
  (56 shorter events, 2.2 us)
Async XLA Ops:
  8.0 72.6 %copy-start = (bf16[1,256,4096]{2,1,0:T(8,128)(2,1)S(1)}, bf16[1,256,4096]{2,1,0:T(8,128)(2,1)}, u32[]{:S(2)}) copy-start(bf16[1,256,4096]{2,1,0:T(8,128)(2,1)} %param.12) | copy-start | bytes 6291460
  8.0 2.6 copy-start.2
  8.0 72.6 %all-gather.5.cloned.1.call-start = ((), (), s32[]{:S(2)}) async-start(), calls=%async_computation.8 | async-start | bytes 3276800 | tf_op jit(solution)/shard_map/all_gather | solution.py:53
  10.6 2.7 copy-start.3
  17.5 45.9 %copy-start.8 = (bf16[128,1024]{1,0:T(8,128)(2,1)S(1)}, bf16[128,1024]{1,0:T(8,128)(2,1)}, u32[]{:S(2)}) copy-start(bf16[128,1024]{1,0:T(8,128)(2,1)} %param.15) | copy-start | bytes 786436
  42.0 80.0 %all-gather.3.cloned.1.call-start = ((), (), s32[]{:S(2)}) async-start(), calls=%async_computation.7 | async-start | bytes 3276800 | tf_op jit(solution)/shard_map/all_gather | solution.py:54
  63.3 280.3 %reduce-scatter.2.cloned.1.call-start = ((), (), s32[]{:S(2)}) async-start(), calls=%async_computation.9 | async-start | bytes 4718592 | tf_op jit(solution)/shard_map/reduce_scatter | solution.py:101
  66.2 0.7 copy-start.10
  80.6 2.8 copy-start.4
  80.6 3.2 copy-start.6
  125.4 1.6 copy-start.7
  219.2 39.7 %all-to-all-start.3 = ((bf16[4,2,163840]{2,1,0:T(2,128)(2,1)}), bf16[4,2,163840]{2,1,0:T(2,128)(2,1)}, u32[]{:S(2)}, u32[]{:S(2)}) async-start(bf16[4,2,163840]{2,1,0:T(2,128)(2,1)} %reshape.387), calls=%async_computation.3 | async-start | bytes 5242880 | tf_op jit(solution)/shard_map/all_to_all | solution.py:88
  224.0 30.4 %collective-permute-start = (f32[1,320]{1,0:T(1,128)S(1)}, f32[1,320]{1,0:T(1,128)S(1)}, u32[]{:S(2)}, u32[]{:S(2)}) collective-permute-start(f32[1,320]{1,0:T(1,128)S(1)} %reduce_sum.58), channel_id=1, source_target_pairs={{0,1},{1,0},{2,3},{3,2},{4,5},{5,4},{6,7},{7,6},{8,9},{9,8},{10,11... | collective-permute-start | bytes 3848 | tf_op jit(solution)/shard_map/ppermute | solution.py:11
  254.4 3.6 %collective-permute-start.1 = (f32[1,320]{1,0:T(1,128)S(1)}, f32[1,320]{1,0:T(1,128)S(1)}, u32[]{:S(2)}, u32[]{:S(2)}) collective-permute-start(f32[1,320]{1,0:T(1,128)S(1)} %reshape_add_fusion), channel_id=1, source_target_pairs={{0,2},{1,3},{2,0},{3,1},{4,6},{5,7},{6,4},{7,5},{8,10},{9,11},{10,... | collective-permute-start | bytes 3848 | tf_op jit(solution)/shard_map/ppermute | solution.py:11
  258.9 41.2 %all-to-all-start.5 = ((f32[1,1,320]{1,0,2:T(1,128)}), f32[1,1,320]{1,0,2:T(1,128)S(1)}, u32[]{:S(2)}, u32[]{:S(2)}) async-start(f32[1,1,320]{1,0,2:T(1,128)} %copy.59), calls=%async_computation.5 | async-start | bytes 327680 | tf_op jit(solution)/shard_map/all_to_all | solution.py:94
  298.1 7.1 %copy-start.9 = (s32[128,2]{0,1:T(2,128)S(1)}, s32[128,2]{0,1:T(2,128)}, u32[]{:S(2)}) copy-start(s32[128,2]{0,1:T(2,128)} %param.10) | copy-start | bytes 3076
  300.1 37.3 %all-to-all-start.4 = ((f32[1,1,320,1024]{3,1,0,2:T(1,128)}), f32[1,1,320,1024]{3,1,0,2:T(1,128)S(1)}, u32[]{:S(2)}, u32[]{:S(2)}) async-start(f32[1,1,320,1024]{3,1,0,2:T(1,128)} %broadcast_in_dim.47), calls=%async_computation.4 | async-start | bytes 2621440 | tf_op jit(solution)/shard_map/all_to_all | solution.py:93
  309.8 4.5 %copy-start.5 = (bf16[1,1,320,4096]{3,2,1,0:T(8,128)(2,1)S(1)}, bf16[1,1,320,4096]{3,2,1,0:T(8,128)(2,1)}, u32[]{:S(2)}) copy-start(bf16[1,1,320,4096]{3,2,1,0:T(8,128)(2,1)} %all-gather.3.cloned.1.call-done) | copy-start | bytes 7864324
  337.6 6.0 %copy-start.1 = (bf16[1,256,4096]{2,1,0:T(8,128)(2,1)S(1)}, bf16[1,256,4096]{2,1,0:T(8,128)(2,1)}, u32[]{:S(2)}) copy-start(bf16[1,256,4096]{2,1,0:T(8,128)(2,1)} %param.12) | copy-start | bytes 6291460
Sparse Core Ops, SparseCore 0:
  42.1 38.4 all-gather.4
  82.5 39.4 all-gather.2
Sparse Core Ops, SparseCore 1:
  66.7 48.8 reduce-scatter.1
